TPU v7x, 32 devices: a whole 2x2x4 slice. The times are simulated.
32 devices in a mesh: sp: 8 (over z, x), tp: 4 (over y, core).
Axes of the slice: x: 2, y: 2, z: 4, core: 2. Of those that a mesh axis runs over, the one named last changes fastest.
Arguments:
- tokens: bfloat16 [2, 128, 1024], P(None, 'sp', 'tp'), may hold values from -6 to 6
- in_weight: bfloat16 [3, 1024, 2048], P(None, 'sp', 'tp'), may hold values from -0.1875 to 0.1875
- gate_weight: bfloat16 [3, 1024, 2048], P(None, 'sp', 'tp'), may hold values from -0.1875 to 0.1875
- out_weight: bfloat16 [3, 2048, 1024], P(None, 'tp', 'sp'), may hold values from -0.25 to 0.25
- recur_weight: bfloat16 [3, 2, 16, 128, 128], P(None, None, 'tp'), may hold values from -0.5 to 0.5
- input_weight: bfloat16 [3, 2, 16, 128, 128], P(None, None, 'tp'), may hold values from -0.5 to 0.5
- conv_taps: bfloat16 [3, 4, 2048], P(None, None, 'tp'), may hold values from -3 to 3
- decay_rate: float32 [3, 2, 2048], P(None, None, 'tp'), may hold values from 0.02 to 0.25
- norm_gain: float32 [3, 1024], replicated, may hold values from 0.5 to 1.5
Outputs:
- mixed_out: bfloat16 [2, 128, 1024], P(None, 'sp', 'tp')
All inputs are finite; a program needn't handle non-finite values.
Results may differ from a plain program's by a relative error of at most 0.04.
Values may be sent and summed in bfloat16 or wider, within the bound.
A program may use at most 64 MiB of HBM per device.

v0:
```python
import jax
import jax.numpy as jnp
from jax import lax
from jax.sharding import PartitionSpec as P

LAYERS = 3
epsilon = 1e-06
gate_power = 8.0


def extended(array, sides, width, wrap):
    for axis, dim in sides:
        size, length = (lax.axis_size(axis), array.shape[dim])
        up = [(i, (i + 1) % size) for i in range(size if wrap else size - 1)]
        down = [(j, i) for i, j in up]
        last = lax.slice_in_dim(array, length - width, length, axis=dim)
        initial = lax.slice_in_dim(array, 0, width, axis=dim)
        before = lax.ppermute(last, axis, up)
        after = lax.ppermute(initial, axis, down)
        array = jnp.concatenate([before, array, after], axis=dim)
    return array


def carried_in(value, axis, join, neutral, backward):
    count, mine = (lax.axis_size(axis), lax.axis_index(axis))
    pieces = jax.tree.map(lambda part: lax.all_gather(part, axis), value)
    if backward:
        pieces = jax.tree.map(lambda part: part[::-1], pieces)
        mine = count - 1 - mine
    subtotal = jax.tree.map(
        lambda part, zero: jnp.full_like(part, 0) + jnp.asarray(zero, part.dtype), value, neutral
    )

    def hop(position, subtotal):
        longer = join(subtotal, jax.tree.map(lambda part: part[position], pieces))
        return jax.tree.map(lambda new, old: jnp.where(position < mine, new, old), longer, subtotal)

    return lax.fori_loop(0, count - 1, hop, subtotal)


def combine(earlier, later_pair):
    first_decay, first_drive = earlier
    second_decay, second_drive = later_pair
    return (first_decay * second_decay, second_decay * first_drive + second_drive)


def body(
    tokens,
    in_weight,
    gate_weight,
    out_weight,
    recur_weight,
    input_weight,
    conv_taps,
    decay_rate,
    norm_gain,
):
    batch_size, tok_rows, _ = tokens.shape
    seq_len = tok_rows * lax.axis_size("sp")
    chan_width = in_weight.shape[2]
    in_whole, gate_whole = (
        lax.all_gather(in_weight, "sp", axis=1, tiled=True),
        lax.all_gather(gate_weight, "sp", axis=1, tiled=True),
    )
    out_whole = lax.all_gather(out_weight, "sp", axis=2, tiled=True)
    state = tokens
    for layer_index in range(LAYERS):
        gathered = lax.all_gather(state, "tp", axis=2, tiled=True)
        flat_rows = gathered.reshape(batch_size * tok_rows, -1).astype(jnp.float32)
        scale_rows = lax.rsqrt(jnp.mean(flat_rows * flat_rows, axis=-1, keepdims=True) + epsilon)
        normed = (flat_rows * scale_rows * norm_gain[layer_index]).astype(jnp.bfloat16)
        branch = jnp.dot(normed, in_whole[layer_index], preferred_element_type=jnp.float32)
        gate_branch = jnp.dot(normed, gate_whole[layer_index], preferred_element_type=jnp.float32)
        branch = branch.astype(jnp.bfloat16).reshape(batch_size, tok_rows, chan_width)
        gate_branch = gate_branch.astype(jnp.bfloat16).reshape(batch_size, tok_rows, chan_width)
        padded = extended(branch, (("sp", 1),), 2, False)
        tap_values = conv_taps[layer_index].astype(jnp.float32)
        conv_out = padded[:, 0:tok_rows].astype(jnp.float32) * tap_values[0]
        for tap_index in range(1, tap_values.shape[0]):
            conv_out = (
                conv_out
                + padded[:, tap_index : tap_index + tok_rows].astype(jnp.float32)
                * tap_values[tap_index]
            )
        conv_out = conv_out.astype(jnp.bfloat16)
        conv_float = conv_out.astype(jnp.float32)
        recur_full = recur_weight[layer_index]
        input_full = input_weight[layer_index]
        heads_local = recur_full.shape[1]
        head_dim = recur_full.shape[2]
        blocks = conv_out.reshape(batch_size, tok_rows, heads_local, head_dim)
        hidden_sum = jnp.zeros((batch_size, tok_rows, chan_width), jnp.float32)
        identity = (
            jnp.ones((batch_size, chan_width), jnp.float32),
            jnp.zeros((batch_size, chan_width), jnp.float32),
        )
        for direction in range(2):
            recur_gate = jax.nn.sigmoid(
                jnp.einsum(
                    "bthd,hde->bthe",
                    blocks,
                    recur_full[direction],
                    preferred_element_type=jnp.float32,
                )
            ).reshape(batch_size, tok_rows, chan_width)
            input_gate = jax.nn.sigmoid(
                jnp.einsum(
                    "bthd,hde->bthe",
                    blocks,
                    input_full[direction],
                    preferred_element_type=jnp.float32,
                )
            ).reshape(batch_size, tok_rows, chan_width)
            log_decay = -gate_power * recur_gate * decay_rate[layer_index, direction] / seq_len
            decay_step = jnp.exp(log_decay)
            driven = jnp.sqrt(-jnp.expm1(2.0 * log_decay)) * input_gate * conv_float
            backward = direction == 1
            cum_decay, cum_drive = lax.associative_scan(
                combine, (decay_step, driven), axis=1, reverse=backward
            )
            if backward:
                totals = (cum_decay[:, 0], cum_drive[:, 0])
                incoming = carried_in(totals, "sp", combine, identity, True)
            else:
                totals = (cum_decay[:, -1], cum_drive[:, -1])
                incoming = carried_in(totals, "sp", combine, identity, False)
            hidden_sum = hidden_sum + (cum_decay * incoming[1][:, None, :] + cum_drive)
        mixed_rows = (hidden_sum * jax.nn.silu(gate_branch.astype(jnp.float32))).astype(
            jnp.bfloat16
        )
        mixed_rows = mixed_rows.reshape(batch_size * tok_rows, chan_width)
        partial_terms = jnp.dot(
            mixed_rows, out_whole[layer_index], preferred_element_type=jnp.float32
        )
        shard_sum = lax.psum_scatter(
            partial_terms.astype(jnp.bfloat16), "tp", scatter_dimension=1, tiled=True
        ).astype(jnp.float32)
        state = shard_sum.astype(jnp.bfloat16).reshape(batch_size, tok_rows, -1)
    return state


def solution(mesh):
    in_specs = (
        P(None, "sp", "tp"),
        P(None, "sp", "tp"),
        P(None, "sp", "tp"),
        P(None, "tp", "sp"),
        P(None, None, "tp", None, None),
        P(None, None, "tp", None, None),
        P(None, None, "tp"),
        P(None, None, "tp"),
        P(),
    )
    out_specs = P(None, "sp", "tp")
    return jax.shard_map(body, mesh=mesh, in_specs=in_specs, out_specs=out_specs, check_vma=False)
```

profile of v0, /device:TPU:0, one launch (start us, length us, event | category | flops | bytes accessed | tf_op | source)
XLA Modules:
  0.0 657.9 jit_solution(7241306334868398253)
XLA Ops:
  6.5 0.7 all-gather.16.cloned.1.call-update
  8.8 1.4 slice_multiply_fusion.7
  10.2 1.4 fusion.178
  11.6 0.7 slice_convert_fusion
  12.4 6.5 all_gather.54
  19.1 53.2 %all-gather.16.cloned.1.call-done = bf16[3,1024,512]{2,1,0:T(8,128)(2,1)} async-done(((bf16[3,128,512]{2,1,0:T(8,128)(2,1)}), bf16[3,1024,512]{2,1,0:T(8,128)(2,1)}) %all-gather.16.cloned.1.call-update) | async-done | bytes 3145744 | tf_op jit(solution)/shard_map/all_gather | solution.py:62
  72.3 1.5 convolution_convert_fusion.8
  73.8 1.3 collective-permute-start.1
  75.1 4.5 collective-permute-start
  79.7 53.5 %all-gather.18.cloned.1.call-done = bf16[3,1024,512]{2,1,0:T(8,128)(2,1)} async-done(((bf16[3,128,512]{2,1,0:T(8,128)(2,1)}), bf16[3,1024,512]{2,1,0:T(8,128)(2,1)}) %all-gather.18.cloned.1.call-update) | async-done | bytes 3145744 | tf_op jit(solution)/shard_map/all_gather | solution.py:63
  133.2 1.5 convolution_convert_fusion.7
  138.2 30.9 %all-gather.2 = f32[16,1,512]{2,1,0:T(1,128)S(1)} all-gather(f32[2,1,512]{2,1,0:T(1,128)S(1)} %slice_add_fusion.19), channel_id=4, replica_groups=mesh['sp'=8,'tp'=4] {'sp'}, dimensions={0}, use_global_device_ids=true | all-gather | bytes 36864 | tf_op jit(solution)/shard_map/all_gather | solution.py:26
  169.2 31.4 %all-gather.3 = f32[16,1,512]{2,1,0:T(1,128)S(1)} all-gather(f32[2,1,512]{2,1,0:T(1,128)S(1)} %slice_add_fusion.16), channel_id=5, replica_groups=mesh['sp'=8,'tp'=4] {'sp'}, dimensions={0}, use_global_device_ids=true | all-gather | bytes 36864 | tf_op jit(solution)/shard_map/all_gather | solution.py:26
  201.5 30.6 %all-gather = f32[16,1,512]{2,1,0:T(1,128)S(1)} all-gather(f32[2,1,512]{2,1,0:T(1,128)S(1)} %slice_add_fusion.23), channel_id=2, replica_groups=mesh['sp'=8,'tp'=4] {'sp'}, dimensions={0}, use_global_device_ids=true | all-gather | bytes 36864 | tf_op jit(solution)/shard_map/all_gather | solution.py:26
  232.2 30.6 %all-gather.1 = f32[16,1,512]{2,1,0:T(1,128)S(1)} all-gather(f32[2,1,512]{2,1,0:T(1,128)S(1)} %slice_add_fusion.20), channel_id=3, replica_groups=mesh['sp'=8,'tp'=4] {'sp'}, dimensions={0}, use_global_device_ids=true | all-gather | bytes 36864 | tf_op jit(solution)/shard_map/all_gather | solution.py:26
  263.6 2.1 convolution_convert_fusion.2
  266.4 17.8 %reduce-scatter.4.cloned.1.call-done = bf16[32,256]{1,0:T(8,128)(2,1)} async-done(((bf16[32,1024]{1,0:T(8,128)(2,1)}), bf16[32,256]{1,0:T(8,128)(2,1)}) %reduce-scatter.4.cloned.1.call-update) | async-done | bytes 16400 | tf_op jit(solution)/shard_map/reduce_scatter | solution.py:135
  284.2 5.4 all_gather.62
  289.9 1.5 convolution_convert_fusion.6
  291.4 1.3 collective-permute-start.3
  292.7 4.5 collective-permute-start.2
  297.3 2.1 convolution_convert_fusion.5
  302.0 1.2 fusion.37
  306.9 32.5 %all-gather.6 = f32[16,1,512]{2,1,0:T(1,128)S(1)} all-gather(f32[2,1,512]{2,1,0:T(1,128)S(1)} %slice_add_fusion.11), channel_id=8, replica_groups=mesh['sp'=8,'tp'=4] {'sp'}, dimensions={0}, use_global_device_ids=true | all-gather | bytes 36864 | tf_op jit(solution)/shard_map/all_gather | solution.py:26
  339.6 30.6 %all-gather.7 = f32[16,1,512]{2,1,0:T(1,128)S(1)} all-gather(f32[2,1,512]{2,1,0:T(1,128)S(1)} %slice_add_fusion.8), channel_id=9, replica_groups=mesh['sp'=8,'tp'=4] {'sp'}, dimensions={0}, use_global_device_ids=true | all-gather | bytes 36864 | tf_op jit(solution)/shard_map/all_gather | solution.py:26
  371.7 0.8 add_multiply_fusion.7
  374.0 30.6 %all-gather.4 = f32[16,1,512]{2,1,0:T(1,128)S(1)} all-gather(f32[2,1,512]{2,1,0:T(1,128)S(1)} %slice_add_fusion.15), channel_id=6, replica_groups=mesh['sp'=8,'tp'=4] {'sp'}, dimensions={0}, use_global_device_ids=true | all-gather | bytes 36864 | tf_op jit(solution)/shard_map/all_gather | solution.py:26
  405.3 0.7 pad.347
  406.0 32.0 %all-gather.5 = f32[16,1,512]{2,1,0:T(1,128)} all-gather(f32[2,1,512]{2,1,0:T(1,128)S(1)} %slice_add_fusion.12), channel_id=7, replica_groups=mesh['sp'=8,'tp'=4] {'sp'}, dimensions={0}, use_global_device_ids=true | all-gather | bytes 36864 | tf_op jit(solution)/shard_map/all_gather | solution.py:26
  438.0 1.4 reduce.8
  439.5 1.4 reshape.296
  440.9 5.0 while.86
  441.6 0.7 fusion.231
  442.3 0.7 fusion.231
  445.2 0.7 fusion.231
  445.9 0.8 fusion.100
  446.7 0.9 convolution_convert_fusion.1
  447.7 17.9 %reduce-scatter.6.cloned.1.call-done = bf16[32,256]{1,0:T(8,128)(2,1)} async-done(((bf16[32,1024]{1,0:T(8,128)(2,1)}), bf16[32,256]{1,0:T(8,128)(2,1)}) %reduce-scatter.6.cloned.1.call-update) | async-done | bytes 16400 | tf_op jit(solution)/shard_map/reduce_scatter | solution.py:135
  465.7 5.4 all_gather.67
  471.2 0.8 fusion.62
  472.0 1.5 convolution_convert_fusion.4
  473.5 1.3 collective-permute-start.5
  474.8 4.7 collective-permute-start.4
  479.6 2.1 convolution_convert_fusion.3
  481.7 0.7 add_convert_fusion
  482.4 1.1 fusion.17
  483.5 1.1 fusion.13
  484.6 1.1 fusion.9
  487.7 1.1 fusion.21
  488.8 0.7 multiply_exponential_fusion.1
  492.6 32.3 %all-gather.10 = f32[16,1,512]{2,1,0:T(1,128)S(1)} all-gather(f32[2,1,512]{2,1,0:T(1,128)S(1)} %slice_add_fusion.3), channel_id=12, replica_groups=mesh['sp'=8,'tp'=4] {'sp'}, dimensions={0}, use_global_device_ids=true | all-gather | bytes 36864 | tf_op jit(solution)/shard_map/all_gather | solution.py:26
  525.1 30.6 %all-gather.11 = f32[16,1,512]{2,1,0:T(1,128)S(1)} all-gather(f32[2,1,512]{2,1,0:T(1,128)S(1)} %slice_add_fusion), channel_id=13, replica_groups=mesh['sp'=8,'tp'=4] {'sp'}, dimensions={0}, use_global_device_ids=true | all-gather | bytes 36864 | tf_op jit(solution)/shard_map/all_gather | solution.py:26
  557.1 0.8 add_multiply_fusion.3
  559.4 30.6 %all-gather.8 = f32[16,1,512]{2,1,0:T(1,128)S(1)} all-gather(f32[2,1,512]{2,1,0:T(1,128)S(1)} %slice_add_fusion.7), channel_id=10, replica_groups=mesh['sp'=8,'tp'=4] {'sp'}, dimensions={0}, use_global_device_ids=true | all-gather | bytes 36864 | tf_op jit(solution)/shard_map/all_gather | solution.py:26
  590.8 0.7 pad.379
  591.5 32.2 %all-gather.9 = f32[16,1,512]{2,1,0:T(1,128)} all-gather(f32[2,1,512]{2,1,0:T(1,128)S(1)} %slice_add_fusion.4), channel_id=11, replica_groups=mesh['sp'=8,'tp'=4] {'sp'}, dimensions={0}, use_global_device_ids=true | all-gather | bytes 36864 | tf_op jit(solution)/shard_map/all_gather | solution.py:26
  623.7 1.4 reduce.12
  625.2 1.4 reshape.300
  626.6 5.0 while.88
  628.7 0.7 fusion.233
  630.1 0.7 fusion.233
  631.6 0.8 fusion.99
  632.4 0.9 convolution_convert_fusion
  633.3 17.8 %reduce-scatter.8.cloned.1.call-done = bf16[32,256]{1,0:T(8,128)(2,1)} async-done(((bf16[32,1024]{1,0:T(8,128)(2,1)}), bf16[32,256]{1,0:T(8,128)(2,1)}) %reduce-scatter.8.cloned.1.call-update) | async-done | bytes 16400 | tf_op jit(solution)/shard_map/reduce_scatter | solution.py:135
  (472 shorter events, 32.3 us)
Async XLA Ops:
  6.5 128.2 %copy-start.3 = (bf16[3,2,4,128,128]{4,3,2,1,0:T(8,128)(2,1)S(1)}, bf16[3,2,4,128,128]{4,3,2,1,0:T(8,128)(2,1)}, u32[]{:S(2)}) copy-start(bf16[3,2,4,128,128]{4,3,2,1,0:T(8,128)(2,1)} %param.26) | copy-start | bytes 2359300
  6.5 128.6 %copy-start.4 = (bf16[3,2,4,128,128]{4,3,2,1,0:T(8,128)(2,1)S(1)}, bf16[3,2,4,128,128]{4,3,2,1,0:T(8,128)(2,1)}, u32[]{:S(2)}) copy-start(bf16[3,2,4,128,128]{4,3,2,1,0:T(8,128)(2,1)} %param.25) | copy-start | bytes 2359300
  6.5 65.8 %all-gather.16.cloned.1.call-start = ((), (), s32[]{:S(2)}) async-start(), calls=%async_computation.3 | async-start | bytes 3538944 | tf_op jit(solution)/shard_map/all_gather | solution.py:62
  7.3 125.9 %all-gather.18.cloned.1.call-start = ((), (), s32[]{:S(2)}) async-start(), calls=%async_computation.4 | async-start | bytes 3538944 | tf_op jit(solution)/shard_map/all_gather | solution.py:63
  8.0 255.6 %all-gather.20.cloned.1.call-start = ((), (), s32[]{:S(2)}) async-start(), calls=%async_computation.5 | async-start | bytes 3538944 | tf_op jit(solution)/shard_map/all_gather | solution.py:65
  8.7 275.5 %reduce-scatter.4.cloned.1.call-start = ((), (), s32[]{:S(2)}) async-start(), calls=%async_computation.6 | async-start | bytes 81920 | tf_op jit(solution)/shard_map/reduce_scatter | solution.py:135
  73.8 60.9 %collective-permute-start.1 = (bf16[2,2,512]{2,1,0:T(2,128)(2,1)S(1)}, bf16[2,2,512]{2,1,0:T(2,128)(2,1)S(1)}, u32[]{:S(2)}, u32[]{:S(2)}) collective-permute-start(bf16[2,2,512]{2,1,0:T(2,128)(2,1)S(1)} %get-tuple-element.783), channel_id=1, source_target_pairs={{4,0},{8,4},{12,8},{16,12},{20,16},{24,20},{28,24},{5,1},{9,5},{13... | collective-permute-start | bytes 12296 | tf_op jit(solution)/shard_map/ppermute | solution.py:19
  75.1 59.6 %collective-permute-start = (bf16[2,2,512]{2,1,0:T(2,128)(2,1)S(1)}, bf16[2,2,512]{2,1,0:T(2,128)(2,1)S(1)}, u32[]{:S(2)}, u32[]{:S(2)}) collective-permute-start(bf16[2,2,512]{2,1,0:T(2,128)(2,1)S(1)} %get-tuple-element.784), channel_id=1, source_target_pairs={{0,4},{4,8},{8,12},{12,16},{16,20},{20,24},{24,28},{1,5},{5,9},{9,... | collective-permute-start | bytes 12296 | tf_op jit(solution)/shard_map/ppermute | solution.py:18
  265.8 199.9 %reduce-scatter.6.cloned.1.call-start = ((), (), s32[]{:S(2)}) async-start(), calls=%async_computation.7 | async-start | bytes 81920 | tf_op jit(solution)/shard_map/reduce_scatter | solution.py:135
  291.4 8.0 %collective-permute-start.3 = (bf16[2,2,512]{2,1,0:T(2,128)(2,1)S(1)}, bf16[2,2,512]{2,1,0:T(2,128)(2,1)S(1)}, u32[]{:S(2)}, u32[]{:S(2)}) collective-permute-start(bf16[2,2,512]{2,1,0:T(2,128)(2,1)S(1)} %get-tuple-element.773), channel_id=1, source_target_pairs={{4,0},{8,4},{12,8},{16,12},{20,16},{24,20},{28,24},{5,1},{9,5},{13... | collective-permute-start | bytes 12296 | tf_op jit(solution)/shard_map/ppermute | solution.py:19
  292.7 6.7 %collective-permute-start.2 = (bf16[2,2,512]{2,1,0:T(2,128)(2,1)S(1)}, bf16[2,2,512]{2,1,0:T(2,128)(2,1)S(1)}, u32[]{:S(2)}, u32[]{:S(2)}) collective-permute-start(bf16[2,2,512]{2,1,0:T(2,128)(2,1)S(1)} %get-tuple-element.774), channel_id=1, source_target_pairs={{0,4},{4,8},{8,12},{12,16},{16,20},{20,24},{24,28},{1,5},{5,9},{9,... | collective-permute-start | bytes 12296 | tf_op jit(solution)/shard_map/ppermute | solution.py:18
  301.8 144.9 %copy-start = (bf16[3,512,1024]{2,1,0:T(8,128)(2,1)S(1)}, bf16[3,512,1024]{2,1,0:T(8,128)(2,1)}, u32[]{:S(2)}) copy-start(bf16[3,512,1024]{2,1,0:T(8,128)(2,1)} %all-gather.20.cloned.1.call-done) | copy-start | bytes 9437188
  370.9 110.8 %copy-start.2 = (f32[1,1,512]{2,1,0:T(1,128)S(1)}, f32[1,1,512]{2,1,0:T(1,128)}, u32[]{:S(2)}) copy-start(f32[1,1,512]{2,1,0:T(1,128)} %get-tuple-element.857) | copy-start | bytes 6148
  405.3 80.4 %copy-start.1 = (f32[1,1,512]{2,1,0:T(1,128)S(1)}, f32[1,1,512]{2,1,0:T(1,128)}, u32[]{:S(2)}) copy-start(f32[1,1,512]{2,1,0:T(1,128)} %get-tuple-element.841) | copy-start | bytes 6148
  447.7 203.4 %reduce-scatter.8.cloned.1.call-start = ((), (), s32[]{:S(2)}) async-start(), calls=%async_computation.8 | async-start | bytes 81920 | tf_op jit(solution)/shard_map/reduce_scatter | solution.py:135
  473.5 8.2 %collective-permute-start.5 = (bf16[2,2,512]{2,1,0:T(2,128)(2,1)S(1)}, bf16[2,2,512]{2,1,0:T(2,128)(2,1)S(1)}, u32[]{:S(2)}, u32[]{:S(2)}) collective-permute-start(bf16[2,2,512]{2,1,0:T(2,128)(2,1)S(1)} %get-tuple-element.763), channel_id=1, source_target_pairs={{4,0},{8,4},{12,8},{16,12},{20,16},{24,20},{28,24},{5,1},{9,5},{13... | collective-permute-start | bytes 12296 | tf_op jit(solution)/shard_map/ppermute | solution.py:19
  474.8 6.9 %collective-permute-start.4 = (bf16[2,2,512]{2,1,0:T(2,128)(2,1)S(1)}, bf16[2,2,512]{2,1,0:T(2,128)(2,1)S(1)}, u32[]{:S(2)}, u32[]{:S(2)}) collective-permute-start(bf16[2,2,512]{2,1,0:T(2,128)(2,1)S(1)} %get-tuple-element.764), channel_id=1, source_target_pairs={{0,4},{4,8},{8,12},{12,16},{16,20},{20,24},{24,28},{1,5},{5,9},{9,... | collective-permute-start | bytes 12296 | tf_op jit(solution)/shard_map/ppermute | solution.py:18
Sparse Core Ops, SparseCore 0:
  9.5 62.7 all-gather.15
  74.5 58.6 all-gather.17
  135.2 62.0 all-gather.19
  265.9 18.3 reduce-scatter.3
  447.8 17.8 reduce-scatter.5
  633.4 17.6 reduce-scatter.7
where the time goes:
time: 660 us; the launch traced here: 658 us
  blocking collectives  392 us (59%)
  waiting for transfers between devices  162 us (25%)
  other arithmetic  28.7 us (4%)
  matrix products  20.8 us (3%)
  local copies, waits for them, and re-layouts  19.3 us (3%)
  starting transfers between devices  17.9 us (3%)
  between operations  15.6 us (2%)
    all_gather x12, blocking collectives, carried_in(): pieces = jax.tree.map(lambda part: lax.all_gather(part, axis), value)  375 us
    all_gather x1, waiting for transfers between devices, body(): lax.all_gather(gate_weight, 'sp', axis=1, tiled=True)  53.5 us
    reduce_scatter x3, waiting for transfers between devices, body(): lax.psum_scatter(partial_terms.astype(jnp.bfloat16), 'tp', scatter_dimens...  53.5 us
    all_gather x1, waiting for transfers between devices, body(): lax.all_gather(in_weight, 'sp', axis=1, tiled=True)  53.2 us
    all_gather x3, blocking collectives, body(): gathered = lax.all_gather(state, 'tp', axis=2, tiled=True)  17.3 us
    ppermute x3, starting transfers between devices, extended(): before = lax.ppermute(last, axis, up)  13.8 us
  transfers between devices with their start and end apart: 12, of which 5 were waited for; matrix products, arithmetic and copies ran while one was open for 2% of the time, Pallas kernels for 0%

commit v1 on v0

--- a/solution.py
+++ b/solution.py
@@ -6,6 +6,9 @@
 LAYERS = 3
 epsilon = 1e-06
 gate_power = 8.0
+pair_the_digits = lambda unit, row_dim: jnp.concatenate(
+    lax.all_gather(unit, axis_name="sp"), axis=row_dim
+)
 
 
 def extended(array, sides, width, wrap):
@@ -60,7 +63,7 @@
     chan_width = in_weight.shape[2]
     in_whole, gate_whole = (
         lax.all_gather(in_weight, "sp", axis=1, tiled=True),
-        lax.all_gather(gate_weight, "sp", axis=1, tiled=True),
+        pair_the_digits(gate_weight, 1),
     )
     out_whole = lax.all_gather(out_weight, "sp", axis=2, tiled=True)
     state = tokens

time: 660 us -> 636 us (0.964)
  other arithmetic: 28.7 us -> 6.14 us
  waiting for transfers between devices: 162 us -> 182 us
  local copies, waits for them, and re-layouts: 19.3 us -> 10.1 us
    ppermute x3, waiting for transfers between devices: 0.02 us -> 11.9 us  [extended(): after = lax.ppermute(initial, axis, down)]
    select_n x42, other arithmetic: 10.3 us -> 0.73 us  [hop(): jnp.where(position < mine, new, old)]
  transfers between devices with their start and end apart: 12 -> 12, of which waited for: 5 -> 8; matrix products, arithmetic and copies ran while one was open for 2% -> 2% of each run, Pallas kernels for 0% -> 0%
where the time goes in v1:
time: 636 us
  blocking collectives  386 us (61%)
  waiting for transfers between devices  182 us (29%)
  matrix products  20.9 us (3%)
  between operations  15.8 us (2%)
  starting transfers between devices  13.5 us (2%)
  local copies, waits for them, and re-layouts  10.1 us (2%)
    all_gather x12, blocking collectives, carried_in(): pieces = jax.tree.map(lambda part: lax.all_gather(part, axis), value)  369 us
    all_gather x1, waiting for transfers between devices, body(): lax.all_gather(in_weight, 'sp', axis=1, tiled=True)  58.8 us
    reduce_scatter x3, waiting for transfers between devices, body(): lax.psum_scatter(partial_terms.astype(jnp.bfloat16), 'tp', scatter_dimens...  55 us
    all_gather x1, waiting for transfers between devices, lax.all_gather(unit, axis_name='sp')  54.4 us
    all_gather x3, blocking collectives, body(): gathered = lax.all_gather(state, 'tp', axis=2, tiled=True)  17.3 us
  transfers between devices with their start and end apart: 12, of which 8 were waited for; matrix products, arithmetic and copies ran while one was open for 2% of the time, Pallas kernels for 0%

profile of v1, /device:TPU:0, one launch (start us, length us, event | category | flops | bytes accessed | tf_op | source)
XLA Modules:
  0.0 635.6 jit_solution(15332917014940081037)
XLA Ops:
  6.5 0.7 all-gather.21.cloned.1.call-update
  7.3 0.7 all-gather.17.cloned.1.call-update
  8.1 0.7 all-gather.19.cloned.1.call-update
  8.8 6.5 %all_gather.57 = bf16[2,16,1024]{2,1,0:T(8,128)(2,1)S(1)} all-gather(bf16[2,16,256]{2,1,0:T(8,128)(2,1)} %param.21), channel_id=1, replica_groups=mesh['sp'=8,'tp'=4] {'tp'}, dimensions={2}, use_global_device_ids=true | all-gather | bytes 81920 | tf_op jit(solution)/shard_map/all_gather | solution.py:71
  15.3 0.8 fusion.179
  16.3 0.7 slice_convert_fusion
  17.0 0.8 slice_multiply_fusion.7
  17.9 54.4 %all-gather.21.cloned.1.call-done = bf16[24,128,512]{2,1,0:T(8,128)(2,1)} async-done(((bf16[3,128,512]{2,1,0:T(8,128)(2,1)}), bf16[24,128,512]{2,1,0:T(8,128)(2,1)}) %all-gather.21.cloned.1.call-update) | async-done | bytes 3145744 | tf_op jit(solution)/shard_map/all_gather | solution.py:10
  72.3 2.1 fusion.165
  74.4 58.8 %all-gather.17.cloned.1.call-done = bf16[3,1024,512]{2,1,0:T(8,128)(2,1)} async-done(((bf16[3,128,512]{2,1,0:T(8,128)(2,1)}), bf16[3,1024,512]{2,1,0:T(8,128)(2,1)}) %all-gather.17.cloned.1.call-update) | async-done | bytes 3145744 | tf_op jit(solution)/shard_map/all_gather | solution.py:65
  133.2 1.5 convolution_convert_fusion.8
  134.7 2.5 collective-permute-start
  137.2 1.3 collective-permute-start.1
  138.5 0.3 convolution_convert_fusion.7
  138.8 4.3 collective-permute-done.1
  143.1 1.1 fusion.41
  144.2 1.1 fusion.49
  145.3 1.1 fusion.45
  146.3 1.1 fusion.53
  150.9 31.2 %all-gather.2 = f32[16,1,512]{2,1,0:T(1,128)S(1)} all-gather(f32[2,1,512]{2,1,0:T(1,128)S(1)} %slice_add_fusion.19), channel_id=4, replica_groups=mesh['sp'=8,'tp'=4] {'sp'}, dimensions={0}, use_global_device_ids=true | all-gather | bytes 36864 | tf_op jit(solution)/shard_map/all_gather | solution.py:29
  182.2 31.1 %all-gather.3 = f32[16,1,512]{2,1,0:T(1,128)S(1)} all-gather(f32[2,1,512]{2,1,0:T(1,128)S(1)} %slice_add_fusion.16), channel_id=5, replica_groups=mesh['sp'=8,'tp'=4] {'sp'}, dimensions={0}, use_global_device_ids=true | all-gather | bytes 36864 | tf_op jit(solution)/shard_map/all_gather | solution.py:29
  213.5 30.6 %all-gather = f32[16,1,512]{2,1,0:T(1,128)S(1)} all-gather(f32[2,1,512]{2,1,0:T(1,128)S(1)} %slice_add_fusion.23), channel_id=2, replica_groups=mesh['sp'=8,'tp'=4] {'sp'}, dimensions={0}, use_global_device_ids=true | all-gather | bytes 36864 | tf_op jit(solution)/shard_map/all_gather | solution.py:29
  244.2 30.6 %all-gather.1 = f32[16,1,512]{2,1,0:T(1,128)S(1)} all-gather(f32[2,1,512]{2,1,0:T(1,128)S(1)} %slice_add_fusion.20), channel_id=3, replica_groups=mesh['sp'=8,'tp'=4] {'sp'}, dimensions={0}, use_global_device_ids=true | all-gather | bytes 36864 | tf_op jit(solution)/shard_map/all_gather | solution.py:29
  274.9 0.3 while.85
  275.2 0.3 while.84
  275.6 2.1 convolution_convert_fusion.2
  277.8 19.3 %reduce-scatter.4.cloned.1.call-done = bf16[32,256]{1,0:T(8,128)(2,1)} async-done(((bf16[32,1024]{1,0:T(8,128)(2,1)}), bf16[32,256]{1,0:T(8,128)(2,1)}) %reduce-scatter.4.cloned.1.call-update) | async-done | bytes 16400 | tf_op jit(solution)/shard_map/reduce_scatter | solution.py:138
  297.1 5.4 all_gather.66
  302.8 1.5 convolution_convert_fusion.6
  304.3 3.4 collective-permute-start.2
  307.7 1.3 collective-permute-start.3
  309.0 0.3 convolution_convert_fusion.5
  309.3 3.9 collective-permute-done.3
  313.2 0.2 fusion.29
  313.4 1.1 fusion.25
  315.6 0.2 fusion.37
  315.8 1.1 fusion.33
  317.5 0.1 slice.1166
  319.2 30.7 %all-gather.7 = f32[16,1,512]{2,1,0:T(1,128)S(1)} all-gather(f32[2,1,512]{2,1,0:T(1,128)S(1)} %slice_add_fusion.11), channel_id=9, replica_groups=mesh['sp'=8,'tp'=4] {'sp'}, dimensions={0}, use_global_device_ids=true | all-gather | bytes 36864 | tf_op jit(solution)/shard_map/all_gather | solution.py:29
  350.0 30.6 %all-gather.8 = f32[16,1,512]{2,1,0:T(1,128)S(1)} all-gather(f32[2,1,512]{2,1,0:T(1,128)S(1)} %slice_add_fusion.8), channel_id=10, replica_groups=mesh['sp'=8,'tp'=4] {'sp'}, dimensions={0}, use_global_device_ids=true | all-gather | bytes 36864 | tf_op jit(solution)/shard_map/all_gather | solution.py:29
  380.7 0.3 while.87
  381.1 30.6 %all-gather.5 = f32[16,1,512]{2,1,0:T(1,128)S(1)} all-gather(f32[2,1,512]{2,1,0:T(1,128)S(1)} %slice_add_fusion.15), channel_id=7, replica_groups=mesh['sp'=8,'tp'=4] {'sp'}, dimensions={0}, use_global_device_ids=true | all-gather | bytes 36864 | tf_op jit(solution)/shard_map/all_gather | solution.py:29
  411.8 30.6 %all-gather.6 = f32[16,1,512]{2,1,0:T(1,128)S(1)} all-gather(f32[2,1,512]{2,1,0:T(1,128)S(1)} %slice_add_fusion.12), channel_id=8, replica_groups=mesh['sp'=8,'tp'=4] {'sp'}, dimensions={0}, use_global_device_ids=true | all-gather | bytes 36864 | tf_op jit(solution)/shard_map/all_gather | solution.py:29
  442.5 0.3 while.86
  442.9 2.1 convolution_convert_fusion.1
  445.1 17.8 %reduce-scatter.6.cloned.1.call-done = bf16[32,256]{1,0:T(8,128)(2,1)} async-done(((bf16[32,1024]{1,0:T(8,128)(2,1)}), bf16[32,256]{1,0:T(8,128)(2,1)}) %reduce-scatter.6.cloned.1.call-update) | async-done | bytes 16400 | tf_op jit(solution)/shard_map/reduce_scatter | solution.py:138
  463.0 5.4 all_gather.71
  468.6 1.5 convolution_convert_fusion.4
  470.1 3.4 collective-permute-start.4
  473.5 1.5 collective-permute-start.5
  475.0 0.3 convolution_convert_fusion.3
  475.3 3.7 collective-permute-done.5
  479.1 0.2 fusion.13
  479.2 1.1 fusion.9
  481.4 0.2 fusion.21
  481.6 1.1 fusion.17
  485.0 30.7 %all-gather.11 = f32[16,1,512]{2,1,0:T(1,128)S(1)} all-gather(f32[2,1,512]{2,1,0:T(1,128)S(1)} %slice_add_fusion.3), channel_id=13, replica_groups=mesh['sp'=8,'tp'=4] {'sp'}, dimensions={0}, use_global_device_ids=true | all-gather | bytes 36864 | tf_op jit(solution)/shard_map/all_gather | solution.py:29
  515.8 30.6 %all-gather.12 = f32[16,1,512]{2,1,0:T(1,128)S(1)} all-gather(f32[2,1,512]{2,1,0:T(1,128)S(1)} %slice_add_fusion), channel_id=14, replica_groups=mesh['sp'=8,'tp'=4] {'sp'}, dimensions={0}, use_global_device_ids=true | all-gather | bytes 36864 | tf_op jit(solution)/shard_map/all_gather | solution.py:29
  546.6 0.3 while.89
  546.9 30.6 %all-gather.9 = f32[16,1,512]{2,1,0:T(1,128)S(1)} all-gather(f32[2,1,512]{2,1,0:T(1,128)S(1)} %slice_add_fusion.7), channel_id=11, replica_groups=mesh['sp'=8,'tp'=4] {'sp'}, dimensions={0}, use_global_device_ids=true | all-gather | bytes 36864 | tf_op jit(solution)/shard_map/all_gather | solution.py:29
  577.6 30.6 %all-gather.10 = f32[16,1,512]{2,1,0:T(1,128)S(1)} all-gather(f32[2,1,512]{2,1,0:T(1,128)S(1)} %slice_add_fusion.4), channel_id=12, replica_groups=mesh['sp'=8,'tp'=4] {'sp'}, dimensions={0}, use_global_device_ids=true | all-gather | bytes 36864 | tf_op jit(solution)/shard_map/all_gather | solution.py:29
  608.3 0.3 while.88
  608.7 2.1 convolution_convert_fusion
  610.8 17.9 %reduce-scatter.8.cloned.1.call-done = bf16[32,256]{1,0:T(8,128)(2,1)} async-done(((bf16[32,1024]{1,0:T(8,128)(2,1)}), bf16[32,256]{1,0:T(8,128)(2,1)}) %reduce-scatter.8.cloned.1.call-update) | async-done | bytes 16400 | tf_op jit(solution)/shard_map/reduce_scatter | solution.py:138
  (465 shorter events, 11.9 us)
Async XLA Ops:
  6.5 65.7 %all-gather.21.cloned.1.call-start = ((), (), s32[]{:S(2)}) async-start(), calls=%async_computation.8 | async-start | bytes 3538944 | tf_op jit(solution)/shard_map/all_gather | solution.py:10
  7.3 125.9 %all-gather.17.cloned.1.call-start = ((), (), s32[]{:S(2)}) async-start(), calls=%async_computation.3 | async-start | bytes 3538944 | tf_op jit(solution)/shard_map/all_gather | solution.py:65
  8.0 267.6 %all-gather.19.cloned.1.call-start = ((), (), s32[]{:S(2)}) async-start(), calls=%async_computation.4 | async-start | bytes 3538944 | tf_op jit(solution)/shard_map/all_gather | solution.py:68
  8.7 288.4 %reduce-scatter.4.cloned.1.call-start = ((), (), s32[]{:S(2)}) async-start(), calls=%async_computation.5 | async-start | bytes 81920 | tf_op jit(solution)/shard_map/reduce_scatter | solution.py:138
  134.7 4.0 collective-permute-start
  137.2 5.9 collective-permute-start.1
  182.2 131.0 %copy-start = (bf16[3,2,4,128,128]{4,3,2,1,0:T(8,128)(2,1)S(1)}, bf16[3,2,4,128,128]{4,3,2,1,0:T(8,128)(2,1)}, u32[]{:S(2)}) copy-start(bf16[3,2,4,128,128]{4,3,2,1,0:T(8,128)(2,1)} %param.25) | copy-start | bytes 2359300
  277.8 185.2 %reduce-scatter.6.cloned.1.call-start = ((), (), s32[]{:S(2)}) async-start(), calls=%async_computation.6 | async-start | bytes 81920 | tf_op jit(solution)/shard_map/reduce_scatter | solution.py:138
  304.3 5.0 collective-permute-start.2
  307.7 5.5 collective-permute-start.3
  445.0 183.7 %reduce-scatter.8.cloned.1.call-start = ((), (), s32[]{:S(2)}) async-start(), calls=%async_computation.7 | async-start | bytes 81920 | tf_op jit(solution)/shard_map/reduce_scatter | solution.py:138
  470.1 5.1 collective-permute-start.4
  473.5 5.5 collective-permute-start.5
Sparse Core Ops, SparseCore 0:
  9.5 62.7 all-gather.20
  74.5 58.6 all-gather.16
  135.2 61.8 all-gather.18
  277.9 19.2 reduce-scatter.3
  445.2 17.7 reduce-scatter.5
  611.0 17.7 reduce-scatter.7
